TPU v7x, 256 devices: a whole 4x4x8 slice. The times are simulated.
256 devices in a mesh: fs: 64 (over z, y, core), tp: 4 (over x).
Axes of the slice: x: 4, y: 4, z: 8, core: 2. Of those that a mesh axis runs over, the one named last changes fastest.
Arguments:
- tokens: bfloat16 [65536, 2048], P('fs', 'tp'), may hold values from -6 to 6
- norm_gain: float32 [2048], P('fs'), may hold values from 0.1 to 1.9
- up_master: float32 [2048, 4096], P('fs', 'tp'), may hold values from -0.125 to 0.125
- down_master: float32 [4096, 2048], P('fs', 'tp'), may hold values from -0.09375 to 0.09375
Outputs:
- mixed: bfloat16 [65536, 2048], P('fs', 'tp')
- up_ready: bfloat16 [2048, 4096], P(None, 'tp')
- down_ready: bfloat16 [4096, 2048], P('tp')
All inputs are finite; a program needn't handle non-finite values.
Results may differ from a plain program's by a relative error of at most 0.0095.
Values may be sent and summed in bfloat16 or wider, within the bound.
A program may use at most 128 MiB of HBM per device.

v0:
```python
import jax
import jax.numpy as jnp
from jax import lax
from jax.sharding import Mesh
from jax.sharding import PartitionSpec as P

FS = ("fs_0", "fs_1", "fs_2")


def sent_to_all(shard, axis):
    peers = lax.axis_size(axis)
    return lax.all_to_all(
        jnp.broadcast_to(shard[None], (peers, *shard.shape)), axis, 0, 0, tiled=True
    )


def laid_out(pieces, dim):
    lengths = list(pieces.shape[1:])
    lengths[dim] *= pieces.shape[0]
    return jnp.moveaxis(pieces, 0, dim).reshape(lengths)


def gathered_by_axis(shard, axes, dim):
    far, near = axes
    initial = sent_to_all(shard, far)
    pieces = jnp.swapaxes(sent_to_all(initial, near), 0, 1)
    return laid_out(pieces.reshape(-1, *shard.shape), dim)


def gather_directly(shard, axis, dim):
    return laid_out(sent_to_all(shard, axis), dim)


def shards(tokens, norm_gain, up_master, down_master):
    group_size = lax.axis_size("tp")
    group_index = lax.axis_index("tp")
    up_local = (norm_gain[:, None] * up_master).astype(jnp.bfloat16)
    up_ready = gathered_by_axis(up_local, (("fs_0", "fs_1"), "fs_2"), 0)
    down_local = down_master.astype(jnp.bfloat16)
    wide_rows = lax.all_gather(down_local, "tp", axis=1, tiled=True)
    whole_down = lax.all_gather(wide_rows, FS, axis=0, tiled=True)
    row_count = whole_down.shape[0] // group_size
    down_ready = lax.dynamic_slice_in_dim(whole_down, group_index * row_count, row_count, 0)
    features = gather_directly(tokens, "tp", 1)
    values = features.astype(jnp.float32)
    mean_square = jnp.mean(values * values, axis=-1, keepdims=True)
    normed = (values * lax.rsqrt(mean_square + 1e-06)).astype(jnp.bfloat16)
    before = jnp.dot(normed, up_ready, preferred_element_type=jnp.float32)
    hidden = jnp.square(jax.nn.relu(before)).astype(jnp.bfloat16)
    partial_value = jnp.dot(hidden, down_ready, preferred_element_type=jnp.float32)
    mixed = lax.psum_scatter(
        partial_value.astype(jnp.bfloat16), "tp", scatter_dimension=1, tiled=True
    )
    return (mixed, up_ready, down_ready)


def solution(mesh):
    finer = Mesh(mesh.devices.reshape(8, 4, 2, mesh.shape["tp"]), ("fs_0", "fs_1", "fs_2", "tp"))
    placed = (P(FS, "tp"), P(FS), P(FS, "tp"), P(FS, "tp"))
    return jax.shard_map(
        shards,
        mesh=finer,
        in_specs=placed,
        out_specs=(P(FS, "tp"), P(None, "tp"), P("tp", None)),
        check_vma=False,
    )
```

profile of v0, /device:TPU:1, one launch (start us, length us, event | category | flops | bytes accessed | tf_op | source)
XLA Modules:
  0.0 243.9 jit_solution(11935646034167226579)
XLA Ops:
  7.2 0.0 all-gather.2.cloned.1.call-start
  7.2 0.9 convert_element_type.33
  8.1 11.8 %all_gather.6 = bf16[64,2048]{1,0:T(8,128)(2,1)} all-gather(bf16[64,512]{1,0:T(8,128)(2,1)S(1)} %convert_element_type.33), channel_id=1, replica_groups=mesh['fs_0'=8,'fs_1'=4,'fs_2'=2,'tp'=4] {'tp'}, dimensions={1}, use_global_device_ids=true | all-gather | bytes 327680 | tf_op jit(solution)/shard_map/all_gather | solution.py:40
  19.9 0.0 all-gather.2.cloned.1.call-update
  20.0 1.5 copy.9
  21.5 2.6 %broadcast_in_dim.6 = bf16[4,1024,512]{1,2,0:T(8,128)(2,1)} broadcast(bf16[1024,512]{0,1:T(8,128)(2,1)S(1)} %copy.9), dimensions={1,2} | broadcast | bytes 5242880 | tf_op jit(solution)/shard_map/broadcast_in_dim | solution.py:13
  24.0 0.0 copy-start
  24.0 0.0 copy-start.1
  24.0 5.0 %all-to-all-start = ((bf16[4,1024,512]{1,2,0:T(8,128)(2,1)}), bf16[4,1024,512]{1,2,0:T(8,128)(2,1)}, u32[]{:S(2)}, u32[]{:S(2)}) async-start(bf16[4,1024,512]{1,2,0:T(8,128)(2,1)} %broadcast_in_dim.6), calls=%async_computation | async-start | bytes 8388608 | tf_op jit(solution)/shard_map/all_to_all | solution.py:12
  29.0 0.0 copy-done
  29.0 0.0 copy-done.1
  29.0 0.1 multiply_convert_fusion.1
  29.1 44.2 %all-to-all-done = bf16[4,1024,512]{1,2,0:T(8,128)(2,1)} async-done(((bf16[4,1024,512]{1,2,0:T(8,128)(2,1)}), bf16[4,1024,512]{1,2,0:T(8,128)(2,1)}, u32[]{:S(2)}, u32[]{:S(2)}) %all-to-all-start) | async-done | bytes 4194336 | tf_op jit(solution)/shard_map/all_to_all | solution.py:12
  73.4 1.6 broadcast_in_dim.7
  74.9 12.8 %all-to-all-start.1 = ((bf16[32,32,1024]{2,1,0:T(8,128)(2,1)}), bf16[32,32,1024]{2,1,0:T(8,128)(2,1)S(1)}, u32[]{:S(2)}, u32[]{:S(2)}) async-start(bf16[32,32,1024]{2,1,0:T(8,128)(2,1)} %broadcast_in_dim.7), calls=%async_computation.1 | async-start | bytes 4194304 | tf_op jit(solution)/shard_map/all_to_all | solution.py:12
  87.7 0.0 reduce-scatter.2.cloned.1.call-start
  87.8 3.2 %fusion = f32[1024]{0:T(1024)S(1)} fusion(bf16[4,1024,512]{1,2,0:T(8,128)(2,1)} %all-to-all-done), kind=kLoop, calls=%fused_computation.2 | loop fusion | flops 6290432 | bytes 4198400 | tf_op jit(solution)/shard_map/reduce_sum | solution.py:46
  91.0 5.5 %fusion.1 = bf16[4,1024,512]{1,2,0:T(8,128)(2,1)} fusion(bf16[4,1024,512]{1,2,0:T(8,128)(2,1)} %all-to-all-done, f32[1024]{0:T(1024)S(1)} %add_rsqrt_fusion), kind=kLoop, calls=%fused_computation.3 | loop fusion | flops 6291456 | bytes 8392704 | tf_op jit(solution)/shard_map/convert_element_type | solution.py:47
  96.5 61.2 %all-to-all-done.1 = bf16[32,32,1024]{2,1,0:T(8,128)(2,1)S(1)} async-done(((bf16[32,32,1024]{2,1,0:T(8,128)(2,1)}), bf16[32,32,1024]{2,1,0:T(8,128)(2,1)S(1)}, u32[]{:S(2)}, u32[]{:S(2)}) %all-to-all-start.1) | async-done | bytes 2097184 | tf_op jit(solution)/shard_map/all_to_all | solution.py:12
  157.6 0.5 broadcast_in_dim.8
  158.2 13.2 %all_to_all.15 = bf16[2,32,32,1024]{3,2,1,0:T(8,128)(2,1)S(1)} all-to-all(bf16[2,32,32,1024]{3,2,1,0:T(8,128)(2,1)S(1)} %broadcast_in_dim.8), channel_id=1, replica_groups=mesh['fs_0'=8,'fs_1'=4,'fs_2'=2,'tp'=4] {'fs_2'}, dimensions={0} | all-to-all | bytes 8388608 | tf_op jit(solution)/shard_map/all_to_all | solution.py:12
  171.4 2.5 %copy.10 = bf16[2,32,32,1024]{3,2,0,1:T(8,128)(2,1)} copy(bf16[2,32,32,1024]{3,2,1,0:T(8,128)(2,1)S(1)} %all_to_all.15) | data formatting | bytes 8388608 | tf_op jit(solution)/shard_map/all_to_all | solution.py:12
  173.9 0.0 all-gather.2.cloned.1.call-done
  173.9 4.8 %constant_dynamic-slice_fusion = bf16[1024,2048]{1,0:T(8,128)(2,1)} fusion(bf16[4096,2048]{1,0:T(8,128)(2,1)} %all-gather.2.cloned.1.call-done, s32[]{:T(128)S(6)} %select_n.3), kind=kLoop, calls=%fused_computation.8 | loop fusion | bytes 8388612 | tf_op jit(solution)/shard_map/dynamic_slice | solution.py:43
  178.6 14.4 %convolution_convert_fusion = bf16[1024,2048]{1,0:T(8,128)(2,1)} fusion(bf16[1024,2048]{1,0:T(8,128)(2,1)} %constant_dynamic-slice_fusion, bf16[1024,2048]{0,1:T(8,128)(2,1)} %bitcast.11, bf16[2048,1024]{1,0:T(8,128)(2,1)} %bitcast.9), kind=kOutput, calls=%fused_computation.5 | convolution fusion | flops 8595177472 | bytes 16777216 | tf_op jit(solution)/shard_map/dot_general | solution.py:50
  193.0 0.0 reduce-scatter.2.cloned.1.call-update
  193.1 44.0 %reduce-scatter.2.cloned.1.call-done = bf16[1024,512]{1,0:T(8,128)(2,1)} async-done(((bf16[1024,2048]{1,0:T(8,128)(2,1)}), bf16[1024,512]{1,0:T(8,128)(2,1)}) %reduce-scatter.2.cloned.1.call-update) | async-done | bytes 1048592 | tf_op jit(solution)/shard_map/reduce_scatter | solution.py:51
  (1 shorter events, 0.0 us)
Async XLA Ops:
  7.2 166.7 %all-gather.2.cloned.1.call-start = ((), (), s32[]{:S(2)}) async-start(), calls=%async_computation.4 | async-start | bytes 17039360 | tf_op jit(solution)/shard_map/all_gather | solution.py:41
  24.0 5.0 %copy-start = (f32[32,1024]{1,0:T(8,128)S(1)}, f32[32,1024]{1,0:T(8,128)}, u32[]{:S(2)}) copy-start(f32[32,1024]{1,0:T(8,128)} %param.6) | copy-start | bytes 393220
  24.0 5.0 %copy-start.1 = (f32[32]{0:T(128)S(1)}, f32[32]{0:T(128)}, u32[]{:S(2)}) copy-start(f32[32]{0:T(128)} %param.5) | copy-start | bytes 388
  24.0 49.3 %all-to-all-start = ((bf16[4,1024,512]{1,2,0:T(8,128)(2,1)}), bf16[4,1024,512]{1,2,0:T(8,128)(2,1)}, u32[]{:S(2)}, u32[]{:S(2)}) async-start(bf16[4,1024,512]{1,2,0:T(8,128)(2,1)} %broadcast_in_dim.6), calls=%async_computation | async-start | bytes 8388608 | tf_op jit(solution)/shard_map/all_to_all | solution.py:12
  74.9 82.7 %all-to-all-start.1 = ((bf16[32,32,1024]{2,1,0:T(8,128)(2,1)}), bf16[32,32,1024]{2,1,0:T(8,128)(2,1)S(1)}, u32[]{:S(2)}, u32[]{:S(2)}) async-start(bf16[32,32,1024]{2,1,0:T(8,128)(2,1)} %broadcast_in_dim.7), calls=%async_computation.1 | async-start | bytes 4194304 | tf_op jit(solution)/shard_map/all_to_all | solution.py:12
  87.7 149.3 %reduce-scatter.2.cloned.1.call-start = ((), (), s32[]{:S(2)}) async-start(), calls=%async_computation.5 | async-start | bytes 5242880 | tf_op jit(solution)/shard_map/reduce_scatter | solution.py:51
Sparse Core Ops, SparseCore 0:
  20.1 148.1 all-gather.1
  193.2 43.8 reduce-scatter.1
where the time goes:
time: 244 us
  waiting for transfers between devices  149 us (61%)
  blocking collectives  25.1 us (10%)
  starting transfers between devices  17.9 us (7%)
  matrix products  14.4 us (6%)
  between operations  14.1 us (6%)
  local copies, waits for them, and re-layouts  13.4 us (5%)
  other arithmetic  9.67 us (4%)
    all_to_all x2, waiting for transfers between devices, sent_to_all(): lax.all_to_all(jnp.broadcast_to(shard[None], (peers, *shard.shape)), axis...  105 us
    reduce_scatter x1, waiting for transfers between devices, shards(): lax.psum_scatter(partial_value.astype(jnp.bfloat16), 'tp', scatter_dimens...  44 us
    all_to_all x2, starting transfers between devices, sent_to_all(): lax.all_to_all(jnp.broadcast_to(shard[None], (peers, *shard.shape)), axis...  17.8 us
    dot_general x1, matrix products, shards(): jnp.dot(hidden, down_ready, preferred_element_type=jnp.float32)  14.4 us
    all_to_all x1, blocking collectives, sent_to_all(): lax.all_to_all(jnp.broadcast_to(shard[None], (peers, *shard.shape)), axis...  13.2 us
    all_gather x1, blocking collectives, shards(): wide_rows = lax.all_gather(down_local, 'tp', axis=1, tiled=True)  11.8 us
    convert_element_type x1, other arithmetic, shards(): normed = (values * lax.rsqrt(mean_square + 1e-06)).astype(jnp.bfloat16)  5.48 us
  transfers between devices with their start and end apart: 4, of which 3 were waited for; matrix products, arithmetic and copies ran while one was open for 7% of the time, Pallas kernels for 0%

commit v1 on v0

v1 whole, which is shorter than its diff:
```python
import functools

import jax
import jax.numpy as jnp
from jax import lax
from jax.experimental import pallas as pl
from jax.experimental.pallas import tpu as pltpu
from jax.sharding import Mesh
from jax.sharding import PartitionSpec as P

FS = ("z", "y", "c")
NZ, NY, NC, NX = 8, 4, 2, 4
CHUNKS = 4
ROWS = 256
MESH = pl.DeviceIdType.MESH


def kernel(
    tok_ref, gain_ref, up_ref, down_ref,
    mixed_ref, up_out, down_out,
    U, D, dl, X, N, H, PT, R2, RA, RB, MX,
    loc_sem, out_sem, dsc_sem,
    uz_s, uz_r, uy_s, uy_r, up_s, up_r,
    dz_s, dz_r, dy_s, dy_r, dp_s, dp_r,
    tx_s, tx_r, rs_s, rs_r,
):
    x, y, z, c = (lax.axis_index(a) for a in ("x", "y", "z", "c"))
    s = 1 - 2 * c

    def xo(k):
        return lax.rem(x + k * s + 2 * NX, NX)

    def yo(k):
        return lax.rem(y + k * s + 2 * NY, NY)

    def zo(k):
        return lax.rem(z + k * s + 2 * NZ, NZ)

    sent = []

    def send(src, dst, ssem, rsem, dev):
        copy = pltpu.make_async_remote_copy(
            src_ref=src, dst_ref=dst, send_sem=ssem, recv_sem=rsem,
            device_id=dev, device_id_type=MESH,
        )
        copy.start()
        sent.append(copy)

    def arrive(dst, ssem, rsem, dev):
        pltpu.make_async_remote_copy(
            src_ref=dst, dst_ref=dst, send_sem=ssem, recv_sem=rsem,
            device_id=dev, device_id_type=MESH,
        ).wait_recv()

    xp, xm = {"x": xo(1)}, {"x": xo(-1)}
    yp, ym = {"y": yo(1)}, {"y": yo(-1)}
    zp, zm = {"z": zo(1)}, {"z": zo(-1)}
    mate = {"c": 1 - c}
    block = lax.div(z, 2)
    far_z = 2 * x + lax.rem(z, 2)
    turned = {"x": block, "z": far_z}
    away = x != block

    load = pltpu.make_async_copy(tok_ref, X.at[3], loc_sem)
    load.start()

    barrier = pltpu.get_barrier_semaphore()
    for dev in (xp, xm, yp, ym, zp, zm, mate):
        pl.semaphore_signal(barrier, inc=1, device_id=dev, device_id_type=MESH)

    @pl.when(away)
    def _():
        pl.semaphore_signal(barrier, inc=1, device_id=turned, device_id_type=MESH)

    gain = gain_ref[...]
    eye = lax.broadcasted_iota(jnp.int32, (32, 32), 0) == lax.broadcasted_iota(jnp.int32, (32, 32), 1)
    column = jnp.sum(jnp.where(eye, jnp.broadcast_to(gain, (32, 32)), 0.0), axis=1, keepdims=True)
    U[z, y, c] = (column * up_ref[...]).astype(jnp.bfloat16)
    mine = down_ref[...].astype(jnp.bfloat16)
    dl[...] = mine

    @pl.when(jnp.logical_not(away))
    def _():
        D[z, y, c] = mine

    load.wait()

    @pl.when(away)
    def _():
        pl.semaphore_wait(barrier, 8)

    @pl.when(jnp.logical_not(away))
    def _():
        pl.semaphore_wait(barrier, 7)

    def rows(i):
        return pl.ds(i * ROWS, ROWS)

    scatter = pltpu.make_async_remote_copy(
        src_ref=dl, dst_ref=D.at[far_z, y, c], send_sem=dsc_sem.at[0], recv_sem=dsc_sem.at[1],
        device_id=turned, device_id_type=MESH,
    )

    @pl.when(away)
    def _():
        scatter.start()

    u_own = U.at[z, y, c]
    send(u_own, u_own, uz_s.at[0], uz_r.at[0], zp)
    send(u_own, u_own, uz_s.at[4], uz_r.at[4], zm)
    for i in range(CHUNKS):
        send(X.at[3, rows(i)], X.at[0, rows(i)], tx_s.at[0, i], tx_r.at[0, i], xp)
        send(X.at[3, rows(i)], X.at[1, rows(i)], tx_s.at[1, i], tx_r.at[1, i], xm)

    events = []

    def at(time, fn):
        events.append((time, len(events), fn))

    z_offsets = [0, -1, 1, -2, 2, -3, 3, -4]

    def u_row(n):
        zz = zo(z_offsets[n])
        piece = U.at[zz, y, c]
        send(piece, piece, uy_s.at[n, 0], uy_r.at[n, 0], yp)
        send(piece, piece, uy_s.at[n, 1], uy_r.at[n, 1], ym)

    def u_z(n):
        k = z_offsets[n]
        piece = U.at[zo(k), y, c]
        if k < 0:
            arrive(piece, uz_s.at[-k - 1], uz_r.at[-k - 1], zm)
            if k > -4:
                send(piece, piece, uz_s.at[-k], uz_r.at[-k], zp)
        else:
            arrive(piece, uz_s.at[3 + k], uz_r.at[3 + k], zp)
            if k < 3:
                send(piece, piece, uz_s.at[4 + k], uz_r.at[4 + k], zm)
        u_row(n)

    def u_y1(n):
        zz = zo(z_offsets[n])
        left = U.at[zz, yo(-1), c]
        arrive(left, uy_s.at[n, 0], uy_r.at[n, 0], ym)
        send(left, left, uy_s.at[n, 2], uy_r.at[n, 2], yp)
        arrive(U.at[zz, yo(1), c], uy_s.at[n, 1], uy_r.at[n, 1], yp)

    def u_y2(n):
        zz = zo(z_offsets[n])
        arrive(U.at[zz, yo(-2), c], uy_s.at[n, 2], uy_r.at[n, 2], ym)
        full = U.at[zz, :, c]
        send(full, full, up_s.at[zz], up_r.at[zz], mate)

    u_row(0)
    u_tz = [0, 3.2, 3.2, 6.4, 6.4, 9.6, 9.6, 12.8]
    u_t1 = [3.3, 6.8, 7.0, 10.8, 11.0, 14.8, 15.0, 18.0]
    for n in range(NZ):
        if n:
            at(u_tz[n], functools.partial(u_z, n))
        at(u_t1[n], functools.partial(u_y1, n))
        at(u_t1[n] + 3.1, functools.partial(u_y2, n))

    y_offsets = [0, -1, 1, -2]

    def d_row(m):
        piece = D.at[z, yo(y_offsets[m]), c]
        send(piece, piece, dz_s.at[m, 0], dz_r.at[m, 0], zm)
        send(piece, piece, dz_s.at[m, 4], dz_r.at[m, 4], zp)

    def d_own():
        @pl.when(away)
        def _():
            scatter.wait_recv()

        piece = D.at[z, y, c]
        send(piece, piece, dy_s.at[0], dy_r.at[0], yp)
        send(piece, piece, dy_s.at[1], dy_r.at[1], ym)
        d_row(0)

    def d_y1():
        left = D.at[z, yo(-1), c]
        arrive(left, dy_s.at[0], dy_r.at[0], ym)
        send(left, left, dy_s.at[2], dy_r.at[2], yp)
        d_row(1)
        arrive(D.at[z, yo(1), c], dy_s.at[1], dy_r.at[1], yp)
        d_row(2)

    def d_y2():
        arrive(D.at[z, yo(-2), c], dy_s.at[2], dy_r.at[2], ym)
        d_row(3)
        full = D.at[z, :, c]
        send(full, full, dp_s.at[z], dp_r.at[z], mate)

    def d_z(m, k):
        yy = yo(y_offsets[m])
        piece = D.at[zo(k), yy, c]
        if k > 0:
            arrive(piece, dz_s.at[m, k - 1], dz_r.at[m, k - 1], zp)
            if k < 4:
                send(piece, piece, dz_s.at[m, k], dz_r.at[m, k], zm)
        else:
            arrive(piece, dz_s.at[m, 3 - k], dz_r.at[m, 3 - k], zm)
            if k > -3:
                send(piece, piece, dz_s.at[m, 4 - k], dz_r.at[m, 4 - k], zp)
        if m == 3:
            full = D.at[zo(k), :, c]
            send(full, full, dp_s.at[zo(k)], dp_r.at[zo(k)], mate)

    at(5.0, d_own)
    at(9.0, d_y1)
    at(12.2, d_y2)
    d_t = [[8.4, 11.8, 15.2, 18.6], [12.6, 16.4, 20.2, 24.0], [12.8, 16.6, 20.4, 24.2], [15.8, 20.0, 24.6, 28.0]]
    for m in range(NY):
        for k in (1, 2, 3, 4):
            at(d_t[m][k - 1], functools.partial(d_z, m, k))
            if k < 4:
                at(d_t[m][k - 1] + 0.1, functools.partial(d_z, m, -k))

    def x_near(i):
        arrive(X.at[0, rows(i)], tx_s.at[0, i], tx_r.at[0, i], xm)
        send(X.at[0, rows(i)], X.at[2, rows(i)], tx_s.at[2, i], tx_r.at[2, i], xp)

    for i in range(CHUNKS):
        at(7.3 + 5.6 * i, functools.partial(x_near, i))

    for _, _, fn in sorted(events, key=lambda e: e[:2]):
        fn()

    def normalise(i):
        arrive(X.at[1, rows(i)], tx_s.at[1, i], tx_r.at[1, i], xp)
        arrive(X.at[2, rows(i)], tx_s.at[2, i], tx_r.at[2, i], xm)
        owners = (xo(-1), xo(1), xo(2), x)

        @pl.loop(0, ROWS // 32)
        def _(b):
            r = pl.ds(pl.multiple_of(i * ROWS + b * 32, 32), 32)
            values = [X[n, r, :].astype(jnp.float32) for n in range(4)]
            total = sum(jnp.sum(v * v, axis=1, keepdims=True) for v in values)
            scale = lax.rsqrt(total * (1.0 / 2048) + 1e-6)
            for v, owner in zip(values, owners):
                N[r, pl.ds(pl.multiple_of(owner * 512, 512), 512)] = (v * scale).astype(jnp.bfloat16)

    def first(i):
        for n in range(4):
            w = U[:, :, :, :, n * 256:(n + 1) * 256].reshape(2048, 256)
            before = jnp.dot(N[rows(i), :], w, preferred_element_type=jnp.float32)
            before = jnp.maximum(before, 0.0)
            H[:, n * 256:(n + 1) * 256] = (before * before).astype(jnp.bfloat16)

    def second(i):
        for j, (k, buf, sem, dev) in enumerate(((2, R2, 0, xp), (-1, RB, 1, xm), (1, None, 2, None), (0, None, 3, None))):
            cc = xo(k)
            w = D[pl.ds(2 * cc, 2)].reshape(1024, 512)
            PT[i, j] = jnp.dot(H[...], w, preferred_element_type=jnp.float32).astype(jnp.bfloat16)
            if buf is not None:
                send(PT.at[i, j], buf.at[i], rs_s.at[sem, i], rs_r.at[sem, i], dev)

    def relay(i):
        arrive(R2.at[i], rs_s.at[0, i], rs_r.at[0, i], xm)
        PT[i, 2] = (PT[i, 2].astype(jnp.float32) + R2[i].astype(jnp.float32)).astype(jnp.bfloat16)
        send(PT.at[i, 2], RA.at[i], rs_s.at[2, i], rs_r.at[2, i], xp)

    stores = []

    def finish(i):
        arrive(RB.at[i], rs_s.at[1, i], rs_r.at[1, i], xp)
        arrive(RA.at[i], rs_s.at[2, i], rs_r.at[2, i], xm)
        total = PT[i, 3].astype(jnp.float32) + RA[i].astype(jnp.float32) + RB[i].astype(jnp.float32)
        MX[rows(i), :] = total.astype(jnp.bfloat16)
        store = pltpu.make_async_copy(MX.at[rows(i)], mixed_ref.at[rows(i)], out_sem.at[i])
        store.start()
        stores.append(store)

    normalise(0)
    for n in range(NZ):
        full = U.at[n, :, 1 - c]
        arrive(full, up_s.at[n], up_r.at[n], mate)
    store = pltpu.make_async_copy(U, up_out, out_sem.at[4])
    store.start()
    stores.append(store)
    first(0)
    for n in range(NZ):
        full = D.at[n, :, 1 - c]
        arrive(full, dp_s.at[n], dp_r.at[n], mate)
    for n in range(NX):
        store = pltpu.make_async_copy(
            D.at[pl.ds(2 * n, 2)], down_out.at[:, :, :, :, pl.ds(n * 512, 512)], out_sem.at[5 + n]
        )
        store.start()
        stores.append(store)
    second(0)
    for i in range(1, CHUNKS):
        normalise(i)
        first(i)
        second(i)
        relay(i - 1)
        if i > 1:
            finish(i - 2)
    relay(CHUNKS - 1)
    finish(CHUNKS - 2)
    finish(CHUNKS - 1)

    for copy in sent:
        copy.wait_send()

    @pl.when(away)
    def _():
        scatter.wait_send()

    for store in stores:
        store.wait()


def shards(tokens, norm_gain, up_master, down_master):
    bf = jnp.bfloat16
    sem = pltpu.SemaphoreType.DMA
    vmem = pl.BlockSpec(memory_space=pltpu.VMEM)
    hbm = pl.BlockSpec(memory_space=pl.ANY)
    mixed, up, down = pl.pallas_call(
        kernel,
        out_shape=(
            jax.ShapeDtypeStruct((1024, 512), bf),
            jax.ShapeDtypeStruct((NZ, NY, NC, 32, 1024), bf),
            jax.ShapeDtypeStruct((2, NY, NC, 64, 2048), bf),
        ),
        in_specs=[hbm, vmem, vmem, vmem],
        out_specs=(hbm, hbm, hbm),
        scratch_shapes=[
            pltpu.VMEM((NZ, NY, NC, 32, 1024), bf),
            pltpu.VMEM((NZ, NY, NC, 64, 512), bf),
            pltpu.VMEM((64, 512), bf),
            pltpu.VMEM((4, 1024, 512), bf),
            pltpu.VMEM((1024, 2048), bf),
            pltpu.VMEM((ROWS, 1024), bf),
            pltpu.VMEM((CHUNKS, 4, ROWS, 512), bf),
            pltpu.VMEM((CHUNKS, ROWS, 512), bf),
            pltpu.VMEM((CHUNKS, ROWS, 512), bf),
            pltpu.VMEM((CHUNKS, ROWS, 512), bf),
            pltpu.VMEM((1024, 512), bf),
            sem, sem((9,)), sem((2,)),
            sem((7,)), sem((7,)), sem((8, 3)), sem((8, 3)), sem((8,)), sem((8,)),
            sem((4, 7)), sem((4, 7)), sem((3,)), sem((3,)), sem((8,)), sem((8,)),
            sem((3, CHUNKS)), sem((3, CHUNKS)), sem((3, CHUNKS)), sem((3, CHUNKS)),
        ],
        compiler_params=pltpu.CompilerParams(
            collective_id=0, has_side_effects=True, vmem_limit_bytes=48 * 1024 * 1024
        ),
        name="handoff",
    )(tokens, norm_gain.reshape(1, 32), up_master, down_master)
    return mixed, up.reshape(2048, 1024), down.reshape(1024, 2048)


def solution(mesh):
    finer = Mesh(mesh.devices.reshape(NZ, NY, NC, NX), ("z", "y", "c", "x"))
    return jax.shard_map(
        shards,
        mesh=finer,
        in_specs=(P(FS, "x"), P(FS), P(FS, "x"), P(FS, "x")),
        out_specs=(P(FS, "x"), P(None, "x"), P("x", None)),
        check_vma=False,
    )
```

time: 244 us -> 99.4 us (0.41)
  waiting for transfers between devices: 149 us -> 0 us
  Pallas kernels: 0 us -> 86.8 us
  blocking collectives: 25.1 us -> 0 us
  starting transfers between devices: 17.9 us -> 0 us
  matrix products: 14.4 us -> 0 us
  between operations: 14.1 us -> 0.65 us
  other arithmetic: 9.67 us -> 0 us
    all_to_all x2 -> x0, waiting for transfers between devices: 105 us -> none  [sent_to_all(): lax.all_to_all(jnp.broadcast_to(shard[None], (peers, *shard.shape)), axis...]
    pallas_call x0 -> x1, Pallas kernels: none -> 86.8 us  [shards(): pl.pallas_call(kernel, out_shape=(jax.ShapeDtypeStruct((1024, 512), bf),...]
    reduce_scatter x1 -> x0, waiting for transfers between devices: 44 us -> none  [shards(): lax.psum_scatter(partial_value.astype(jnp.bfloat16), 'tp', scatter_dimens...]
    all_to_all x2 -> x0, starting transfers between devices: 17.8 us -> none  [sent_to_all(): lax.all_to_all(jnp.broadcast_to(shard[None], (peers, *shard.shape)), axis...]
    dot_general x1 -> x0, matrix products: 14.4 us -> none  [shards(): jnp.dot(hidden, down_ready, preferred_element_type=jnp.float32)]
    all_to_all x1 -> x0, blocking collectives: 13.2 us -> none  [sent_to_all(): lax.all_to_all(jnp.broadcast_to(shard[None], (peers, *shard.shape)), axis...]
    all_gather x1 -> x0, blocking collectives: 11.8 us -> none  [shards(): wide_rows = lax.all_gather(down_local, 'tp', axis=1, tiled=True)]
    unnamed x5 -> x13, local copies, waits for them, and re-layouts: 1.5 us -> 11.5 us
  transfers between devices with their start and end apart: 4 -> 0, of which waited for: 3 -> 0; matrix products, arithmetic and copies ran while one was open for 7% -> 0% of each run, Pallas kernels for 0% -> 0%
where the time goes in v1:
time: 99.4 us; the launch traced here: 98.9 us
  Pallas kernels  86.8 us (87%)
  local copies, waits for them, and re-layouts  11.5 us (12%)
    pallas_call x1, Pallas kernels, shards(): pl.pallas_call(kernel, out_shape=(jax.ShapeDtypeStruct((1024, 512), bf),...  86.8 us
    unnamed x13, local copies, waits for them, and re-layouts  11.5 us

profile of v1, /device:TPU:1, one launch (start us, length us, event | category | flops | bytes accessed | tf_op | source)
XLA Modules:
  0.0 98.9 jit_solution(12085592860428598272)
XLA Ops:
  0.6 0.0 copy-start
  0.6 1.2 %copy-done = bf16[1024,512]{1,0:T(8,128)(2,1)S(1)} copy-done((bf16[1024,512]{1,0:T(8,128)(2,1)S(1)}, bf16[1024,512]{1,0:T(8,128)(2,1)}, u32[]{:S(2)}) %copy-start) | copy-done | bytes 1048600
  1.9 0.0 copy-start.1
  1.9 0.9 copy-done.1
  2.8 0.0 copy-start.2
  2.8 0.9 copy-done.2
  3.7 0.0 copy-start.3
  3.7 0.7 copy-done.3
  4.3 86.8 %handoff.1 = (bf16[1024,512]{1,0:T(8,128)(2,1)S(1)}, bf16[8,4,2,32,1024]{4,3,2,1,0:T(8,128)(2,1)}, bf16[2,4,2,64,2048]{4,3,2,1,0:T(8,128)(2,1)}) custom-call(bf16[1024,512]{1,0:T(8,128)(2,1)S(1)} %copy-done, f32[1,32]{1,0:T(1,128)S(1)} %bitcast.3, f32[32,1024]{1,0:T(8,128)S(1)} %copy-done.1, f32[64,512]{1,0:T(8,128)S(1)} %copy-done.2), custom_call_target="tpu_custom_call" | custom-call | tf_op jit(solution)/shard_map/handoff/pallas_call | solution.py:319
  91.1 1.0 copy.10
  92.1 0.0 copy-start.4
  92.1 4.8 %copy.11 = bf16[2048,1024]{1,0:T(8,128)(2,1)} copy(bf16[2048,1024]{1,0:T(8,128)(2,1)} %bitcast.5) | data formatting | bytes 8388608
  96.9 0.0 copy-done.4
  96.9 2.0 %copy.12 = bf16[1024,2048]{1,0:T(8,128)(2,1)} copy(bf16[1024,2048]{1,0:T(8,128)(2,1)S(1)} %bitcast.4) | data formatting | bytes 8388608
Async XLA Ops:
  0.6 1.2 %copy-start = (bf16[1024,512]{1,0:T(8,128)(2,1)S(1)}, bf16[1024,512]{1,0:T(8,128)(2,1)}, u32[]{:S(2)}) copy-start(bf16[1024,512]{1,0:T(8,128)(2,1)} %tok_ref.1) | copy-start | bytes 3145732
  1.9 0.9 copy-start.1
  2.8 0.9 copy-start.2
  3.7 0.7 copy-start.3
  92.1 4.8 %copy-start.4 = (bf16[2,4,2,64,2048]{4,3,2,1,0:T(8,128)(2,1)S(1)}, bf16[2,4,2,64,2048]{4,3,2,1,0:T(8,128)(2,1)}, u32[]{:S(2)}) copy-start(bf16[2,4,2,64,2048]{4,3,2,1,0:T(8,128)(2,1)} %get-tuple-element.8) | copy-start | bytes 12582916

commit v2 on v0

v2 whole, which is shorter than its diff:
```python
import jax
import jax.numpy as jnp
from jax import lax
from jax.experimental import pallas as pl
from jax.experimental.pallas import tpu as pltpu
from jax.sharding import Mesh
from jax.sharding import PartitionSpec as P

FS = ("z", "y", "c")
SIZE = {"z": 8, "y": 4, "c": 2, "x": 4}
CHUNKS = 4
ROWS = 256
MESH = pl.DeviceIdType.MESH
WAY = {("y", 1): (0, -1, 1, -2), ("z", 1): (0, -1, 1, -2, 2, -3, 3, -4), ("z", -1): (0, 1, -1, 2, -2, 3, -3, 4), ("y", -1): (0, 1, -1, 2)}
OWN, RING1, RING2, ROW, PASS, NORM, FIRST, SECOND, RELAY, FINISH = range(10)
UP_ORDER = (
    (OWN,), (RING1, -1), (RING1, 1), (RING2, 0, -1), (RING2, 0, 1), (PASS, 0), (RING1, -2), (RING2, 1, -1),
    (RING2, 1, 1), (RING1, 2), (RING2, 2, 1), (RING2, 2, -1), (RING2, 0, -2), (ROW, 0), (RING1, -3), (RING1, 3),
    (RING2, 3, 1), (PASS, 1), (RING2, 3, -1), (RING2, 4, 1), (RING2, 1, -2), (ROW, 1), (RING2, 4, -1), (RING2, 2, 2),
    (ROW, 2), (RING1, -4), (RING2, 5, -1), (RING2, 5, 1), (PASS, 2), (RING2, 6, -1), (RING2, 6, 1), (RING2, 4, -2),
    (ROW, 4), (RING2, 3, 2), (ROW, 3), (RING2, 7, -1), (RING2, 7, 1), (RING2, 5, -2), (ROW, 5), (RING2, 6, 2),
    (ROW, 6), (PASS, 3), (RING2, 7, 2), (ROW, 7), (NORM, 0), (FIRST, 0), (NORM, 1), (FIRST, 1), (NORM, 2), (FIRST, 2),
    (SECOND, 0, 0), (SECOND, 0, 1), (SECOND, 0, 2), (SECOND, 0, 3), (SECOND, 1, 0), (SECOND, 1, 1), (SECOND, 1, 2),
    (SECOND, 1, 3), (SECOND, 2, 0), (SECOND, 2, 1), (SECOND, 2, 2), (SECOND, 2, 3), (NORM, 3), (FIRST, 3),
    (SECOND, 3, 0), (SECOND, 3, 1), (RELAY, 0), (SECOND, 3, 2), (SECOND, 3, 3), (RELAY, 1), (RELAY, 2), (RELAY, 3),
    (FINISH, 0), (FINISH, 1), (FINISH, 2), (FINISH, 3),
)
DOWN_ORDER = (
    (OWN,), (PASS, 0), (RING2, 0, 1), (RING1, 1), (RING2, 0, -1), (RING1, -1), (PASS, 1), (RING2, 0, 2),
    (RING2, 1, -1), (RING2, 1, 1), (RING1, 2), (ROW, 0), (RING2, 0, -2), (RING2, 2, 1), (PASS, 2), (RING2, 0, 3),
    (RING2, 2, -1), (RING2, 1, 2), (RING2, 1, -2), (RING2, 3, 1), (ROW, 2), (RING2, 3, -1), (ROW, 1), (RING2, 2, 2),
    (RING2, 0, -3), (PASS, 3), (RING2, 1, 3), (RING2, 2, -2), (RING2, 3, 2), (ROW, 4), (RING2, 1, -3), (NORM, 0),
    (RING2, 2, 3), (RING2, 3, -2), (ROW, 3), (RING2, 0, -4), (RING2, 3, 3), (ROW, 6), (RING2, 2, -3), (RING2, 2, 4),
    (RING2, 1, -4), (RING2, 3, 4), (ROW, 7), (RING2, 3, -3), (ROW, 5), (FIRST, 0), (SECOND, 0, 0), (SECOND, 0, 1),
    (SECOND, 0, 2), (SECOND, 0, 3), (NORM, 1), (FIRST, 1), (SECOND, 1, 0), (SECOND, 1, 1), (SECOND, 1, 2),
    (SECOND, 1, 3), (NORM, 2), (FIRST, 2), (SECOND, 2, 0), (RELAY, 0), (SECOND, 2, 1), (SECOND, 2, 2), (SECOND, 2, 3),
    (NORM, 3), (FIRST, 3), (SECOND, 3, 0), (SECOND, 3, 1), (SECOND, 3, 2), (SECOND, 3, 3), (RELAY, 1), (RELAY, 2),
    (FINISH, 0), (RELAY, 3), (FINISH, 1), (FINISH, 2), (FINISH, 3),
)


def kernel(
    tok_ref, gain_ref, up_ref, down_ref,
    MX, U, D,
    gv, uv, dv, ul, dl, X, N, H, PT, R2, RA, RB,
    loc_sem, dsc_sem,
    u1_s, u1_r, u2_s, u2_r, um_s, um_r,
    d1_s, d1_r, d2_s, d2_r, dm_s, dm_r,
    tx_s, tx_r, rs_s, rs_r,
):
    place = {a: lax.axis_index(a) for a in ("x", "y", "z", "c")}
    x, y, z, c = (place[a] for a in ("x", "y", "z", "c"))
    turn = 1 - 2 * c

    def step(axis, k):
        return lax.rem(place[axis] + k * turn + 2 * SIZE[axis], SIZE[axis])

    def near(axis, k):
        return {axis: step(axis, k)}

    sent = []

    def send(src, dst, ssem, rsem, dev):
        copy = pltpu.make_async_remote_copy(
            src_ref=src, dst_ref=dst, send_sem=ssem, recv_sem=rsem,
            device_id=dev, device_id_type=MESH,
        )
        copy.start()
        sent.append(copy)

    def arrive(dst, ssem, rsem, dev):
        pltpu.make_async_remote_copy(
            src_ref=dst, dst_ref=dst, send_sem=ssem, recv_sem=rsem,
            device_id=dev, device_id_type=MESH,
        ).wait_recv()

    mate = {"c": 1 - c}
    block = lax.div(z, 2)
    far_z = 2 * x + lax.rem(z, 2)
    away = x != block
    leaves = jnp.logical_or(away, c == 0)

    loads = [
        pltpu.make_async_copy(src, dst, loc_sem.at[n])
        for n, (src, dst) in enumerate(((gain_ref, gv), (up_ref, uv), (down_ref, dv), (tok_ref, X.at[3])))
    ]
    for load in loads:
        load.start()

    barrier = pltpu.get_barrier_semaphore()
    for dev in (*(near(a, k) for a in ("x", "y", "z") for k in (1, -1)), mate):
        pl.semaphore_signal(barrier, inc=1, device_id=dev, device_id_type=MESH)

    @pl.when(jnp.logical_and(away, c == 1))
    def _():
        for n in (0, 1):
            pl.semaphore_signal(
                barrier, inc=1, device_id={"x": block, "z": far_z, "c": n}, device_id_type=MESH
            )

    for load in loads[:3]:
        load.wait()
    eye = lax.broadcasted_iota(jnp.int32, (32, 32), 0) == lax.broadcasted_iota(jnp.int32, (32, 32), 1)
    column = jnp.sum(jnp.where(eye, jnp.broadcast_to(gv[...], (32, 32)), 0.0), axis=1, keepdims=True)
    up_mine = (column * uv[...]).astype(jnp.bfloat16)
    ul[...] = up_mine

    @pl.when(c == 0)
    def _():
        U[z, y, 0] = up_mine

    mine = dv[...].astype(jnp.bfloat16)
    dl[...] = mine

    @pl.when(jnp.logical_not(leaves))
    def _():
        D[z, y, c] = mine

    loads[3].wait()

    @pl.when(away)
    def _():
        pl.semaphore_wait(barrier, 8)

    @pl.when(jnp.logical_not(away))
    def _():
        pl.semaphore_wait(barrier, 7)

    def rows(i):
        return pl.ds(i * ROWS, ROWS)

    def stream(events, buf, axes, way1, ways2, s1, r1, s2, r2, sm, rm):

        def piece(k1, k2):
            at = {axes[0]: step(axes[0], k1), axes[1]: step(axes[1], k2)}
            return buf.at[at["z"], at["y"]]

        def hop(way, axis, k, ref, ss, rr):
            for d in (1, -1):
                if (k * d > 0 or k == 0) and k + d in way:
                    n = way.index(k + d) - 1
                    send(ref, ref, ss(n), rr(n), near(axis, -d))

        def hop1(k):
            hop(way1, axes[0], k, piece(k, 0), lambda n: s1.at[n], lambda n: r1.at[n])

        def hop2(i, k):
            hop(ways2[i], axes[1], k, piece(way1[i], k), lambda n: s2.at[i, n], lambda n: r2.at[i, n])

        def own():
            hop1(0)
            hop2(0, 0)

        def take1(i):
            k, n = way1[i], i - 1
            arrive(piece(k, 0), s1.at[n], r1.at[n], near(axes[0], 1))
            hop1(k)
            hop2(i, 0)

        def take2(i, n):
            k = ways2[i][n + 1]
            arrive(piece(way1[i], k), s2.at[i, n], r2.at[i, n], near(axes[1], 1))
            hop2(i, k)

        def row(n):
            zz = step("z", (way1 if axes[0] == "z" else WAY["z", 1])[n])
            send(buf.at[zz], buf.at[zz], sm.at[n], rm.at[zz], mate)

        for i in range(1, len(way1)):
            events[RING1, way1[i]] = lambda i=i: take1(i)
        for i in range(len(way1)):
            for n in range(len(ways2[i]) - 1):
                events[RING2, i, ways2[i][n + 1]] = lambda i=i, n=n: take2(i, n)
        for n in range(8):
            events[ROW, n] = lambda n=n: row(n)

        def complete():
            for n in range(8):
                arrive(buf.at[n], sm.at[n], rm.at[n], mate)

        return own, complete

    up_events, down_events, events = {}, {}, {}
    up_ways = [WAY["y", w] for w in (1, 1, -1, -1) * 2]
    down_ways = [WAY["z", w] for w in (1, 1, -1, -1)]
    up_own, up_complete = stream(up_events, U, "zy", WAY["z", 1], up_ways, u1_s, u1_r, u2_s, u2_r, um_s, um_r)
    down_own, down_complete = stream(down_events, D, "yz", WAY["y", -1], down_ways, d1_s, d1_r, d2_s, d2_r, dm_s, dm_r)

    scatter = pltpu.make_async_remote_copy(
        src_ref=dl, dst_ref=D.at[far_z, y, c], send_sem=dsc_sem.at[2], recv_sem=dsc_sem.at[c],
        device_id={"x": block, "z": far_z, "c": 1}, device_id_type=MESH,
    )
    give = pltpu.make_async_remote_copy(
        src_ref=ul, dst_ref=U.at[z, y, 1], send_sem=dsc_sem.at[3], recv_sem=dsc_sem.at[3],
        device_id={"c": 0}, device_id_type=MESH,
    )

    def scattered(n):
        arrive(D.at[z, y, n], dsc_sem.at[2], dsc_sem.at[n], mate)

    def up_here():
        give.wait_recv()
        up_own()

    def down_here():
        scattered(0)

        @pl.when(away)
        def _():
            scattered(1)

        down_own()

    def token(src, slot, i, k):
        send(X.at[src, rows(i)], X.at[slot, rows(i)], tx_s.at[slot, i], tx_r.at[slot, i], near("x", k))

    def token_in(slot, i):
        arrive(X.at[slot, rows(i)], tx_s.at[slot, i], tx_r.at[slot, i], near("x", 1))

    @pl.when(leaves)
    def _():
        scatter.start()

    def pass_on(i):
        token_in(0, i)
        token(0, 2, i, 1)

    def normalise(i):
        token_in(1, i)
        token_in(2, i)
        owners = (step("x", -1), step("x", 1), step("x", 2), x)

        @pl.loop(0, ROWS // 32)
        def _(b):
            r = pl.ds(pl.multiple_of(i * ROWS + b * 32, 32), 32)
            values = [X[n, r, :].astype(jnp.float32) for n in range(4)]
            total = sum(jnp.sum(v * v, axis=1, keepdims=True) for v in values)
            scale = lax.rsqrt(total * (1.0 / 2048) + 1e-6)
            for v, owner in zip(values, owners):
                N[r, pl.ds(pl.multiple_of(owner * 512, 512), 512)] = (v * scale).astype(jnp.bfloat16)

    def first(i, core):
        if i == 0 and core == 1:
            up_complete()
        for n in range(4):
            w = U[:, :, :, :, n * 256:(n + 1) * 256].reshape(2048, 256)
            before = jnp.dot(N[rows(i), :], w, preferred_element_type=jnp.float32)
            before = jnp.maximum(before, 0.0)
            H[rows(i), n * 256:(n + 1) * 256] = (before * before).astype(jnp.bfloat16)

    def second(i, j, core):
        if i == 0 and j == 0 and core == 0:
            down_complete()
        k, buf, n = ((2, R2, 0), (-1, RB, 1), (1, None, 2), (0, None, 3))[j]
        w = D[pl.ds(2 * step("x", k), 2)].reshape(1024, 512)
        PT[i, j] = jnp.dot(H[rows(i), :], w, preferred_element_type=jnp.float32).astype(jnp.bfloat16)
        if buf is not None:
            send(PT.at[i, j], buf.at[i], rs_s.at[n, i], rs_r.at[n, i], near("x", 1 if j == 0 else -1))

    def relay(i):
        arrive(R2.at[i], rs_s.at[0, i], rs_r.at[0, i], near("x", 1))
        PT[i, 2] = (PT[i, 2].astype(jnp.float32) + R2[i].astype(jnp.float32)).astype(jnp.bfloat16)
        send(PT.at[i, 2], RA.at[i], rs_s.at[2, i], rs_r.at[2, i], near("x", 1))

    def finish(i):
        arrive(RB.at[i], rs_s.at[1, i], rs_r.at[1, i], near("x", 1))
        arrive(RA.at[i], rs_s.at[2, i], rs_r.at[2, i], near("x", 1))
        total = PT[i, 3].astype(jnp.float32) + RA[i].astype(jnp.float32) + RB[i].astype(jnp.float32)
        MX[rows(i), :] = total.astype(jnp.bfloat16)

    for i in range(CHUNKS):
        events[PASS, i] = lambda i=i: pass_on(i)
        events[NORM, i] = lambda i=i: normalise(i)
        events[RELAY, i] = lambda i=i: relay(i)
        events[FINISH, i] = lambda i=i: finish(i)

    def program(core, order):
        todo = events | (down_events if core else up_events) | {(OWN,): down_here if core else up_here}
        for i in range(CHUNKS):
            todo[FIRST, i] = lambda i=i: first(i, core)
            for j in range(4):
                todo[SECOND, i, j] = lambda i=i, j=j: second(i, j, core)
        if core == 1:
            give.start()
        for i in range(CHUNKS):
            token(3, 0, i, 1)
            token(3, 1, i, -1)
        for name in order:
            todo[name]()
        for copy in sent:
            copy.wait_send()
        if core == 1:
            give.wait_send()
        sent.clear()

    @pl.when(c == 0)
    def _():
        program(0, UP_ORDER)

    @pl.when(c == 1)
    def _():
        program(1, DOWN_ORDER)

    @pl.when(leaves)
    def _():
        scatter.wait_send()


def write(mixed_ref, up_ref, down_ref, mixed_out, up_out, down_out, sems):
    copies = [pltpu.make_async_copy(up_ref, up_out, sems.at[0])]
    for n in range(4):
        copies.append(pltpu.make_async_copy(
            down_ref.at[pl.ds(2 * n, 2)], down_out.at[:, :, :, :, pl.ds(n * 512, 512)], sems.at[1 + n]
        ))
    copies.append(pltpu.make_async_copy(mixed_ref, mixed_out, sems.at[5]))
    for copy in copies:
        copy.start()
    for copy in copies:
        copy.wait()


def shards(tokens, norm_gain, up_master, down_master):
    bf = jnp.bfloat16
    f32 = jnp.float32
    sem = pltpu.SemaphoreType.DMA
    vmem = pl.BlockSpec(memory_space=pltpu.VMEM)
    hbm = pl.BlockSpec(memory_space=pltpu.HBM)
    arguments = [
        pltpu.with_memory_space_constraint(v, pltpu.HBM)
        for v in (tokens, norm_gain.reshape(1, 32), up_master, down_master)
    ]
    mixed, up, down = pl.pallas_call(
        kernel,
        out_shape=(
            jax.ShapeDtypeStruct((1024, 512), bf),
            jax.ShapeDtypeStruct((8, 4, 2, 32, 1024), bf),
            jax.ShapeDtypeStruct((8, 4, 2, 64, 512), bf),
        ),
        in_specs=[hbm, hbm, hbm, hbm],
        out_specs=(vmem, vmem, vmem),
        scratch_shapes=[
            pltpu.VMEM((1, 32), f32),
            pltpu.VMEM((32, 1024), f32),
            pltpu.VMEM((64, 512), f32),
            pltpu.VMEM((32, 1024), bf),
            pltpu.VMEM((64, 512), bf),
            pltpu.VMEM((4, 1024, 512), bf),
            pltpu.VMEM((1024, 2048), bf),
            pltpu.VMEM((1024, 1024), bf),
            pltpu.VMEM((CHUNKS, 4, ROWS, 512), bf),
            pltpu.VMEM((CHUNKS, ROWS, 512), bf),
            pltpu.VMEM((CHUNKS, ROWS, 512), bf),
            pltpu.VMEM((CHUNKS, ROWS, 512), bf),
            sem((4,)), sem((4,)),
            sem((7,)), sem((7,)), sem((8, 3)), sem((8, 3)), sem((8,)), sem((8,)),
            sem((3,)), sem((3,)), sem((4, 7)), sem((4, 7)), sem((8,)), sem((8,)),
            sem((3, CHUNKS)), sem((3, CHUNKS)), sem((3, CHUNKS)), sem((3, CHUNKS)),
        ],
        compiler_params=pltpu.CompilerParams(
            collective_id=0, has_side_effects=True, vmem_limit_bytes=40 * 1024 * 1024
        ),
        name="handoff",
    )(*arguments)
    mixed, up, down = pl.pallas_call(
        write,
        out_shape=(
            jax.ShapeDtypeStruct((1024, 512), bf),
            jax.ShapeDtypeStruct((8, 4, 2, 32, 1024), bf),
            jax.ShapeDtypeStruct((2, 4, 2, 64, 2048), bf),
        ),
        in_specs=[vmem, vmem, vmem],
        out_specs=(hbm, hbm, hbm),
        scratch_shapes=[sem((6,))],
        compiler_params=pltpu.CompilerParams(vmem_limit_bytes=16 * 1024 * 1024),
        name="write",
    )(mixed, up, down)
    return mixed, up.reshape(2048, 1024), down.reshape(1024, 2048)


def solution(mesh):
    finer = Mesh(mesh.devices.reshape(8, 4, 2, 4), ("z", "y", "c", "x"))
    return jax.shard_map(
        shards,
        mesh=finer,
        in_specs=(P(FS, "x"), P(FS), P(FS, "x"), P(FS, "x")),
        out_specs=(P(FS, "x"), P(None, "x"), P("x", None)),
        check_vma=False,
    )
```

time: 244 us -> 88 us (0.36)
  waiting for transfers between devices: 149 us -> 0 us
  Pallas kernels: 0 us -> 87.1 us
  blocking collectives: 25.1 us -> 0 us
  starting transfers between devices: 17.9 us -> 0 us
  matrix products: 14.4 us -> 0 us
  local copies, waits for them, and re-layouts: 13.4 us -> 0 us
  between operations: 14.1 us -> 0.8 us
  other arithmetic: 9.67 us -> 0 us
    all_to_all x2 -> x0, waiting for transfers between devices: 105 us -> none  [sent_to_all(): lax.all_to_all(jnp.broadcast_to(shard[None], (peers, *shard.shape)), axis...]
    pallas_call x0 -> x2, Pallas kernels: none -> 87.1 us  [the longest x1 83.5 us: shards(): pl.pallas_call(kernel, out_shape=(jax.ShapeDtypeStruct((1024, 512), bf),...]
    reduce_scatter x1 -> x0, waiting for transfers between devices: 44 us -> none  [shards(): lax.psum_scatter(partial_value.astype(jnp.bfloat16), 'tp', scatter_dimens...]
    all_to_all x2 -> x0, starting transfers between devices: 17.8 us -> none  [sent_to_all(): lax.all_to_all(jnp.broadcast_to(shard[None], (peers, *shard.shape)), axis...]
    dot_general x1 -> x0, matrix products: 14.4 us -> none  [shards(): jnp.dot(hidden, down_ready, preferred_element_type=jnp.float32)]
    all_to_all x1 -> x0, blocking collectives: 13.2 us -> none  [sent_to_all(): lax.all_to_all(jnp.broadcast_to(shard[None], (peers, *shard.shape)), axis...]
    all_gather x1 -> x0, blocking collectives: 11.8 us -> none  [shards(): wide_rows = lax.all_gather(down_local, 'tp', axis=1, tiled=True)]
    convert_element_type x3 -> x0, other arithmetic: 6.48 us -> none  [the longest x1 5.48 us: shards(): normed = (values * lax.rsqrt(mean_square + 1e-06)).astype(jnp.bfloat16)]
  transfers between devices with their start and end apart: 4 -> 0, of which waited for: 3 -> 0; matrix products, arithmetic and copies ran while one was open for 7% -> 0% of each run, Pallas kernels for 0% -> 0%
where the time goes in v2:
time: 88 us; the launch traced here: 87.9 us
  Pallas kernels  87.1 us (99%)
    pallas_call x1, Pallas kernels, shards(): pl.pallas_call(kernel, out_shape=(jax.ShapeDtypeStruct((1024, 512), bf),...  83.5 us
    pallas_call x1, Pallas kernels, shards(): pl.pallas_call(write, out_shape=(jax.ShapeDtypeStruct((1024, 512), bf), j...  3.67 us

profile of v2, /device:TPU:1, one launch (start us, length us, event | category | flops | bytes accessed | tf_op | source)
XLA Modules:
  0.0 87.9 jit_solution(10065671143031704760)
XLA Ops:
  0.6 83.5 %handoff.1 = (bf16[1024,512]{1,0:T(8,128)(2,1)S(1)}, bf16[8,4,2,32,1024]{4,3,2,1,0:T(8,128)(2,1)S(1)}, bf16[8,4,2,64,512]{4,3,2,1,0:T(8,128)(2,1)S(1)}) custom-call(bf16[1024,512]{1,0:T(8,128)(2,1)} %tok_ref.1, f32[1,32]{1,0:T(1,128)} %bitcast.3, f32[32,1024]{1,0:T(8,128)} %up_ref.1, f32[64,512]{1,0:T(8,128)} %down_ref.1), custom_call_target="tpu_custom_call" | custom-call | tf_op jit(solution)/shard_map/handoff/pallas_call | solution.py:332
  84.1 3.7 %write.1 = (bf16[1024,512]{1,0:T(8,128)(2,1)}, bf16[8,4,2,32,1024]{4,3,2,1,0:T(8,128)(2,1)}, bf16[2,4,2,64,2048]{4,3,2,1,0:T(8,128)(2,1)}) custom-call(bf16[1024,512]{1,0:T(8,128)(2,1)S(1)} %get-tuple-element.9.mixed_ref, bf16[8,4,2,32,1024]{4,3,2,1,0:T(8,128)(2,1)S(1)} %get-tuple-element.10.up_ref, bf16[8,4,2,64,512]{4,3,2,1,0:T(8,128)(2,1)S(1)} %get-tuple-element.11.down_ref), custom_call_target="tpu_custom_call" | custom-call | tf_op jit(solution)/shard_map/write/pallas_call | solution.py:364

commit v3 on v2

--- a/solution.py
+++ b/solution.py
@@ -19,23 +19,23 @@
     (RING2, 3, 1), (PASS, 1), (RING2, 3, -1), (RING2, 4, 1), (RING2, 1, -2), (ROW, 1), (RING2, 4, -1), (RING2, 2, 2),
     (ROW, 2), (RING1, -4), (RING2, 5, -1), (RING2, 5, 1), (PASS, 2), (RING2, 6, -1), (RING2, 6, 1), (RING2, 4, -2),
     (ROW, 4), (RING2, 3, 2), (ROW, 3), (RING2, 7, -1), (RING2, 7, 1), (RING2, 5, -2), (ROW, 5), (RING2, 6, 2),
-    (ROW, 6), (PASS, 3), (RING2, 7, 2), (ROW, 7), (NORM, 0), (FIRST, 0), (NORM, 1), (FIRST, 1), (NORM, 2), (FIRST, 2),
-    (SECOND, 0, 0), (SECOND, 0, 1), (SECOND, 0, 2), (SECOND, 0, 3), (SECOND, 1, 0), (SECOND, 1, 1), (SECOND, 1, 2),
-    (SECOND, 1, 3), (SECOND, 2, 0), (SECOND, 2, 1), (SECOND, 2, 2), (SECOND, 2, 3), (NORM, 3), (FIRST, 3),
-    (SECOND, 3, 0), (SECOND, 3, 1), (RELAY, 0), (SECOND, 3, 2), (SECOND, 3, 3), (RELAY, 1), (RELAY, 2), (RELAY, 3),
-    (FINISH, 0), (FINISH, 1), (FINISH, 2), (FINISH, 3),
+    (ROW, 6), (PASS, 3), (NORM, 0), (RING2, 7, 2), (ROW, 7), (FIRST, 0), (SECOND, 0, 0), (SECOND, 0, 1),
+    (SECOND, 0, 2), (SECOND, 0, 3), (NORM, 1), (FIRST, 1), (SECOND, 1, 0), (SECOND, 1, 1), (SECOND, 1, 2),
+    (SECOND, 1, 3), (NORM, 2), (FIRST, 2), (SECOND, 2, 0), (SECOND, 2, 1), (SECOND, 2, 2), (SECOND, 2, 3), (RELAY, 0),
+    (NORM, 3), (FIRST, 3), (SECOND, 3, 0), (SECOND, 3, 1), (SECOND, 3, 2), (SECOND, 3, 3), (RELAY, 1), (RELAY, 2),
+    (RELAY, 3), (FINISH, 0), (FINISH, 1), (FINISH, 2), (FINISH, 3),
 )
 DOWN_ORDER = (
     (OWN,), (PASS, 0), (RING2, 0, 1), (RING1, 1), (RING2, 0, -1), (RING1, -1), (PASS, 1), (RING2, 0, 2),
     (RING2, 1, -1), (RING2, 1, 1), (RING1, 2), (ROW, 0), (RING2, 0, -2), (RING2, 2, 1), (PASS, 2), (RING2, 0, 3),
     (RING2, 2, -1), (RING2, 1, 2), (RING2, 1, -2), (RING2, 3, 1), (ROW, 2), (RING2, 3, -1), (ROW, 1), (RING2, 2, 2),
-    (RING2, 0, -3), (PASS, 3), (RING2, 1, 3), (RING2, 2, -2), (RING2, 3, 2), (ROW, 4), (RING2, 1, -3), (NORM, 0),
-    (RING2, 2, 3), (RING2, 3, -2), (ROW, 3), (RING2, 0, -4), (RING2, 3, 3), (ROW, 6), (RING2, 2, -3), (RING2, 2, 4),
-    (RING2, 1, -4), (RING2, 3, 4), (ROW, 7), (RING2, 3, -3), (ROW, 5), (FIRST, 0), (SECOND, 0, 0), (SECOND, 0, 1),
-    (SECOND, 0, 2), (SECOND, 0, 3), (NORM, 1), (FIRST, 1), (SECOND, 1, 0), (SECOND, 1, 1), (SECOND, 1, 2),
-    (SECOND, 1, 3), (NORM, 2), (FIRST, 2), (SECOND, 2, 0), (RELAY, 0), (SECOND, 2, 1), (SECOND, 2, 2), (SECOND, 2, 3),
-    (NORM, 3), (FIRST, 3), (SECOND, 3, 0), (SECOND, 3, 1), (SECOND, 3, 2), (SECOND, 3, 3), (RELAY, 1), (RELAY, 2),
-    (FINISH, 0), (RELAY, 3), (FINISH, 1), (FINISH, 2), (FINISH, 3),
+    (RING2, 0, -3), (PASS, 3), (RING2, 1, 3), (RING2, 2, -2), (RING2, 3, 2), (ROW, 4), (RING2, 1, -3), (RING2, 2, 3),
+    (RING2, 3, -2), (ROW, 3), (NORM, 0), (RING2, 3, 3), (ROW, 6), (RING2, 2, -3), (RING2, 3, -3), (ROW, 5), (FIRST, 0),
+    (SECOND, 0, 0), (SECOND, 0, 1), (SECOND, 0, 2), (RING2, 0, -4), (RING2, 2, 4), (RING2, 1, -4), (RING2, 3, 4),
+    (ROW, 7), (SECOND, 0, 3), (NORM, 1), (FIRST, 1), (SECOND, 1, 0), (SECOND, 1, 1), (SECOND, 1, 2), (SECOND, 1, 3),
+    (NORM, 2), (FIRST, 2), (SECOND, 2, 0), (SECOND, 2, 1), (SECOND, 2, 2), (SECOND, 2, 3), (RELAY, 0), (NORM, 3),
+    (FIRST, 3), (SECOND, 3, 0), (SECOND, 3, 1), (SECOND, 3, 2), (SECOND, 3, 3), (RELAY, 1), (RELAY, 2), (RELAY, 3),
+    (FINISH, 0), (FINISH, 1), (FINISH, 2), (FINISH, 3),
 )
 
 
@@ -44,9 +44,7 @@
     MX, U, D,
     gv, uv, dv, ul, dl, X, N, H, PT, R2, RA, RB,
     loc_sem, dsc_sem,
-    u1_s, u1_r, u2_s, u2_r, um_s, um_r,
-    d1_s, d1_r, d2_s, d2_r, dm_s, dm_r,
-    tx_s, tx_r, rs_s, rs_r,
+    send_sem, ring1_sem, ring2_sem, tx_sem, rs_sem,
 ):
     place = {a: lax.axis_index(a) for a in ("x", "y", "z", "c")}
     x, y, z, c = (place[a] for a in ("x", "y", "z", "c"))
@@ -58,21 +56,20 @@
     def near(axis, k):
         return {axis: step(axis, k)}
 
-    sent = []
-
-    def send(src, dst, ssem, rsem, dev):
-        copy = pltpu.make_async_remote_copy(
-            src_ref=src, dst_ref=dst, send_sem=ssem, recv_sem=rsem,
+    def copy(src, dst, kind, rsem, dev):
+        return pltpu.make_async_remote_copy(
+            src_ref=src, dst_ref=dst, send_sem=send_sem.at[kind], recv_sem=rsem,
             device_id=dev, device_id_type=MESH,
         )
-        copy.start()
-        sent.append(copy)
-
-    def arrive(dst, ssem, rsem, dev):
-        pltpu.make_async_remote_copy(
-            src_ref=dst, dst_ref=dst, send_sem=ssem, recv_sem=rsem,
-            device_id=dev, device_id_type=MESH,
-        ).wait_recv()
+
+    def send(src, dst, kind, rsem, dev):
+        copy(src, dst, kind, rsem, dev).start()
+
+    def sent(whole, kind):
+        copy(whole, whole, kind, send_sem.at[kind], mate).wait_send()
+
+    def arrive(dst, rsem, dev):
+        copy(dst, dst, 0, rsem, dev).wait_recv()
 
     mate = {"c": 1 - c}
     block = lax.div(z, 2)
@@ -129,23 +126,24 @@
     def rows(i):
         return pl.ds(i * ROWS, ROWS)
 
-    def stream(events, buf, axes, way1, ways2, s1, r1, s2, r2, sm, rm):
+    def stream(events, buf, axes, way1, ways2):
 
         def piece(k1, k2):
             at = {axes[0]: step(axes[0], k1), axes[1]: step(axes[1], k2)}
             return buf.at[at["z"], at["y"]]
 
-        def hop(way, axis, k, ref, ss, rr):
+        wide = len(ways2[0]) - 1
+
+        def hop(way, axis, k, ref, kind, sems):
             for d in (1, -1):
                 if (k * d > 0 or k == 0) and k + d in way:
-                    n = way.index(k + d) - 1
-                    send(ref, ref, ss(n), rr(n), near(axis, -d))
+                    send(ref, ref, kind, sems(way.index(k + d) - 1), near(axis, -d))
 
         def hop1(k):
-            hop(way1, axes[0], k, piece(k, 0), lambda n: s1.at[n], lambda n: r1.at[n])
+            hop(way1, axes[0], k, piece(k, 0), 0, lambda n: ring1_sem.at[n])
 
         def hop2(i, k):
-            hop(ways2[i], axes[1], k, piece(way1[i], k), lambda n: s2.at[i, n], lambda n: r2.at[i, n])
+            hop(ways2[i], axes[1], k, piece(way1[i], k), 1, lambda n: ring2_sem.at[i * wide + n])
 
         def own():
             hop1(0)
@@ -153,18 +151,18 @@
 
         def take1(i):
             k, n = way1[i], i - 1
-            arrive(piece(k, 0), s1.at[n], r1.at[n], near(axes[0], 1))
+            arrive(piece(k, 0), ring1_sem.at[n], near(axes[0], 1))
             hop1(k)
             hop2(i, 0)
 
         def take2(i, n):
             k = ways2[i][n + 1]
-            arrive(piece(way1[i], k), s2.at[i, n], r2.at[i, n], near(axes[1], 1))
+            arrive(piece(way1[i], k), ring2_sem.at[i * wide + n], near(axes[1], 1))
             hop2(i, k)
 
         def row(n):
-            zz = step("z", (way1 if axes[0] == "z" else WAY["z", 1])[n])
-            send(buf.at[zz], buf.at[zz], sm.at[n], rm.at[zz], mate)
+            zz = step("z", WAY["z", 1][n])
+            send(buf.at[zz], buf.at[zz], 2, dsc_sem.at[4 + max(n - 1, 0) // 2], mate)
 
         for i in range(1, len(way1)):
             events[RING1, way1[i]] = lambda i=i: take1(i)
@@ -174,17 +172,21 @@
         for n in range(8):
             events[ROW, n] = lambda n=n: row(n)
 
-        def complete():
-            for n in range(8):
-                arrive(buf.at[n], sm.at[n], rm.at[n], mate)
-
-        return own, complete
+        def complete(distance):
+            arrive(buf.at[pl.ds(0, (3, 2, 2, 1)[distance])], dsc_sem.at[4 + distance], mate)
+
+        def all_sent():
+            sent(buf.at[pl.ds(0, len(way1) - 1), 0], 0)
+            sent(buf.at[pl.ds(0, len(way1) * wide // 4)], 1)
+            sent(buf, 2)
+
+        return own, complete, all_sent
 
     up_events, down_events, events = {}, {}, {}
     up_ways = [WAY["y", w] for w in (1, 1, -1, -1) * 2]
     down_ways = [WAY["z", w] for w in (1, 1, -1, -1)]
-    up_own, up_complete = stream(up_events, U, "zy", WAY["z", 1], up_ways, u1_s, u1_r, u2_s, u2_r, um_s, um_r)
-    down_own, down_complete = stream(down_events, D, "yz", WAY["y", -1], down_ways, d1_s, d1_r, d2_s, d2_r, dm_s, dm_r)
+    up_own, up_complete, up_sent = stream(up_events, U, "zy", WAY["z", 1], up_ways)
+    down_own, down_complete, down_sent = stream(down_events, D, "yz", WAY["y", -1], down_ways)
 
     scatter = pltpu.make_async_remote_copy(
         src_ref=dl, dst_ref=D.at[far_z, y, c], send_sem=dsc_sem.at[2], recv_sem=dsc_sem.at[c],
@@ -196,7 +198,7 @@
     )
 
     def scattered(n):
-        arrive(D.at[z, y, n], dsc_sem.at[2], dsc_sem.at[n], mate)
+        arrive(D.at[z, y, n], dsc_sem.at[n], mate)
 
     def up_here():
         give.wait_recv()
@@ -212,10 +214,10 @@
         down_own()
 
     def token(src, slot, i, k):
-        send(X.at[src, rows(i)], X.at[slot, rows(i)], tx_s.at[slot, i], tx_r.at[slot, i], near("x", k))
+        send(X.at[src, rows(i)], X.at[slot, rows(i)], 3, tx_sem.at[slot, i], near("x", k))
 
     def token_in(slot, i):
-        arrive(X.at[slot, rows(i)], tx_s.at[slot, i], tx_r.at[slot, i], near("x", 1))
+        arrive(X.at[slot, rows(i)], tx_sem.at[slot, i], near("x", 1))
 
     @pl.when(leaves)
     def _():
@@ -241,31 +243,41 @@
 
     def first(i, core):
         if i == 0 and core == 1:
-            up_complete()
+            for distance in range(4):
+                up_complete(distance)
         for n in range(4):
             w = U[:, :, :, :, n * 256:(n + 1) * 256].reshape(2048, 256)
             before = jnp.dot(N[rows(i), :], w, preferred_element_type=jnp.float32)
             before = jnp.maximum(before, 0.0)
             H[rows(i), n * 256:(n + 1) * 256] = (before * before).astype(jnp.bfloat16)
 
+    lean = 1 - 2 * lax.rem(z, 2)
+
     def second(i, j, core):
-        if i == 0 and j == 0 and core == 0:
-            down_complete()
-        k, buf, n = ((2, R2, 0), (-1, RB, 1), (1, None, 2), (0, None, 3))[j]
-        w = D[pl.ds(2 * step("x", k), 2)].reshape(1024, 512)
-        PT[i, j] = jnp.dot(H[rows(i), :], w, preferred_element_type=jnp.float32).astype(jnp.bfloat16)
-        if buf is not None:
-            send(PT.at[i, j], buf.at[i], rs_s.at[n, i], rs_r.at[n, i], near("x", 1 if j == 0 else -1))
+        if i == 0 and core == 0:
+            down_complete(j)
+        cc = lax.rem(block + (0, -1, 1, 2)[j] * lean + 4, 4)
+        hops = lax.rem((cc - x) * turn + 8, 4)
+        w = D[pl.ds(2 * cc, 2)].reshape(1024, 512)
+        PT[i, hops] = jnp.dot(H[rows(i), :], w, preferred_element_type=jnp.float32).astype(jnp.bfloat16)
+
+        @pl.when(hops == 2)
+        def _():
+            send(PT.at[i, 2], R2.at[i], 4, rs_sem.at[0, i], near("x", 1))
+
+        @pl.when(hops == 3)
+        def _():
+            send(PT.at[i, 3], RB.at[i], 4, rs_sem.at[1, i], near("x", -1))
 
     def relay(i):
-        arrive(R2.at[i], rs_s.at[0, i], rs_r.at[0, i], near("x", 1))
-        PT[i, 2] = (PT[i, 2].astype(jnp.float32) + R2[i].astype(jnp.float32)).astype(jnp.bfloat16)
-        send(PT.at[i, 2], RA.at[i], rs_s.at[2, i], rs_r.at[2, i], near("x", 1))
+        arrive(R2.at[i], rs_sem.at[0, i], near("x", 1))
+        PT[i, 1] = (PT[i, 1].astype(jnp.float32) + R2[i].astype(jnp.float32)).astype(jnp.bfloat16)
+        send(PT.at[i, 1], RA.at[i], 4, rs_sem.at[2, i], near("x", 1))
 
     def finish(i):
-        arrive(RB.at[i], rs_s.at[1, i], rs_r.at[1, i], near("x", 1))
-        arrive(RA.at[i], rs_s.at[2, i], rs_r.at[2, i], near("x", 1))
-        total = PT[i, 3].astype(jnp.float32) + RA[i].astype(jnp.float32) + RB[i].astype(jnp.float32)
+        arrive(RB.at[i], rs_sem.at[1, i], near("x", 1))
+        arrive(RA.at[i], rs_sem.at[2, i], near("x", 1))
+        total = PT[i, 0].astype(jnp.float32) + RA[i].astype(jnp.float32) + RB[i].astype(jnp.float32)
         MX[rows(i), :] = total.astype(jnp.bfloat16)
 
     for i in range(CHUNKS):
@@ -287,11 +299,13 @@
             token(3, 1, i, -1)
         for name in order:
             todo[name]()
-        for copy in sent:
-            copy.wait_send()
+        sent(X.at[pl.ds(0, 3)], 3)
+        sent(PT.at[pl.ds(0, 3)], 4)
         if core == 1:
+            down_sent()
             give.wait_send()
-        sent.clear()
+        else:
+            up_sent()
 
     @pl.when(c == 0)
     def _():
@@ -307,12 +321,13 @@
 
 
 def write(mixed_ref, up_ref, down_ref, mixed_out, up_out, down_out, sems):
-    copies = [pltpu.make_async_copy(up_ref, up_out, sems.at[0])]
+    copies = [pltpu.make_async_copy(mixed_ref, mixed_out, sems.at[8])]
     for n in range(4):
+        two = pl.ds(2 * n, 2)
+        copies.append(pltpu.make_async_copy(up_ref.at[two], up_out.at[two], sems.at[n]))
         copies.append(pltpu.make_async_copy(
-            down_ref.at[pl.ds(2 * n, 2)], down_out.at[:, :, :, :, pl.ds(n * 512, 512)], sems.at[1 + n]
+            down_ref.at[two], down_out.at[:, :, :, :, pl.ds(n * 512, 512)], sems.at[4 + n]
         ))
-    copies.append(pltpu.make_async_copy(mixed_ref, mixed_out, sems.at[5]))
     for copy in copies:
         copy.start()
     for copy in copies:
@@ -351,10 +366,7 @@
             pltpu.VMEM((CHUNKS, ROWS, 512), bf),
             pltpu.VMEM((CHUNKS, ROWS, 512), bf),
             pltpu.VMEM((CHUNKS, ROWS, 512), bf),
-            sem((4,)), sem((4,)),
-            sem((7,)), sem((7,)), sem((8, 3)), sem((8, 3)), sem((8,)), sem((8,)),
-            sem((3,)), sem((3,)), sem((4, 7)), sem((4, 7)), sem((8,)), sem((8,)),
-            sem((3, CHUNKS)), sem((3, CHUNKS)), sem((3, CHUNKS)), sem((3, CHUNKS)),
+            sem((4,)), sem((8,)), sem((5,)), sem((7,)), sem((28,)), sem((3, CHUNKS)), sem((3, CHUNKS)),
         ],
         compiler_params=pltpu.CompilerParams(
             collective_id=0, has_side_effects=True, vmem_limit_bytes=40 * 1024 * 1024
@@ -370,7 +382,7 @@
         ),
         in_specs=[vmem, vmem, vmem],
         out_specs=(hbm, hbm, hbm),
-        scratch_shapes=[sem((6,))],
+        scratch_shapes=[sem((9,))],
         compiler_params=pltpu.CompilerParams(vmem_limit_bytes=16 * 1024 * 1024),
         name="write",
     )(mixed, up, down)

time: 88 us -> 84.6 us (0.961); the launches traced: 87.9 us -> 83.2 us
  Pallas kernels: 87.1 us -> 82.4 us
    pallas_call x1, Pallas kernels: 83.5 us -> 78.7 us  [shards(): pl.pallas_call(kernel, out_shape=(jax.ShapeDtypeStruct((1024, 512), bf),...]
where the time goes in v3:
time: 84.6 us; the launch traced here: 83.2 us
  Pallas kernels  82.4 us (97%)
    pallas_call x1, Pallas kernels, shards(): pl.pallas_call(kernel, out_shape=(jax.ShapeDtypeStruct((1024, 512), bf),...  78.7 us
    pallas_call x1, Pallas kernels, shards(): pl.pallas_call(write, out_shape=(jax.ShapeDtypeStruct((1024, 512), bf), j...  3.69 us

profile of v3, /device:TPU:1, one launch (start us, length us, event | category | flops | bytes accessed | tf_op | source)
XLA Modules:
  0.0 83.2 jit_solution(54846156910369967)
XLA Ops:
  0.6 78.7 %handoff.1 = (bf16[1024,512]{1,0:T(8,128)(2,1)S(1)}, bf16[8,4,2,32,1024]{4,3,2,1,0:T(8,128)(2,1)S(1)}, bf16[8,4,2,64,512]{4,3,2,1,0:T(8,128)(2,1)S(1)}) custom-call(bf16[1024,512]{1,0:T(8,128)(2,1)} %tok_ref.1, f32[1,32]{1,0:T(1,128)} %bitcast.3, f32[32,1024]{1,0:T(8,128)} %up_ref.1, f32[64,512]{1,0:T(8,128)} %down_ref.1), custom_call_target="tpu_custom_call" | custom-call | tf_op jit(solution)/shard_map/handoff/pallas_call | solution.py:347
  79.3 3.7 %write.1 = (bf16[1024,512]{1,0:T(8,128)(2,1)}, bf16[8,4,2,32,1024]{4,3,2,1,0:T(8,128)(2,1)}, bf16[2,4,2,64,2048]{4,3,2,1,0:T(8,128)(2,1)}) custom-call(bf16[1024,512]{1,0:T(8,128)(2,1)S(1)} %get-tuple-element.9.mixed_ref, bf16[8,4,2,32,1024]{4,3,2,1,0:T(8,128)(2,1)S(1)} %get-tuple-element.10.up_ref, bf16[8,4,2,64,512]{4,3,2,1,0:T(8,128)(2,1)S(1)} %get-tuple-element.11.down_ref), custom_call_target="tpu_custom_call" | custom-call | tf_op jit(solution)/shard_map/write/pallas_call | solution.py:376
